TPU v7x, 32 devices: a whole 2x2x4 slice. The times are simulated.
32 devices in a mesh: sp: 4 (over z), fs: 4 (over y, x), tp: 2 (over core).
Axes of the slice: x: 2, y: 2, z: 4, core: 2. Of those that a mesh axis runs over, the one named last changes fastest.
Arguments:
- tokens: bfloat16 [4, 512, 2048], P('fs', ('sp', 'tp')), may hold values from -6 to 6
- input_norm_gain: float32 [2048], replicated, may hold values from 0.1 to 1.9
- pooling_input_weight: bfloat16 [2048, 1024], P('sp', 'tp'), may hold values from -0.125 to 0.125
- query_weight: bfloat16 [2048, 1024], P('sp', 'tp'), may hold values from -0.125 to 0.125
- forget_weight: bfloat16 [2048, 1024], P('sp', 'tp'), may hold values from -0.125 to 0.125
- value_weight: bfloat16 [2048, 1024], P('sp', 'tp'), may hold values from -0.125 to 0.125
- pooling_group_maps: bfloat16 [4, 256, 256], P('tp'), may hold values from -0.375 to 0.375
- pooling_scale: float32 [1024], P('tp'), may hold values from 0.1 to 1.9
- lower_bound_logits: float32 [1024], P('tp')
- decay_spike: float32 [4, 512, 8], P('fs', 'sp', 'tp'), may hold values from -0.75 to 0
- head_norm_gain: float32 [1024], P('tp'), may hold values from 0.1 to 1.9
- pooling_output_weight: bfloat16 [1024, 2048], P('tp', 'sp'), may hold values from -0.125 to 0.125
- recurrent_output_weight: bfloat16 [1024, 2048], P('tp', 'sp'), may hold values from -0.125 to 0.125
Outputs:
- mixed: bfloat16 [4, 512, 2048], P('fs', ('sp', 'tp'))
All inputs are finite; a program needn't handle non-finite values.
Results may differ from a plain program's by a relative error of at most 0.013.
Values may be sent and summed in bfloat16 or wider, within the bound.
No kernel may reach another device: no remote copies, remote signals or barrier semaphores. Data moves between devices by JAX's collectives and lax.ppermute only.
A program may use at most 64 MiB of HBM per device.

v0:
```python
import jax
import jax.numpy as jnp
from jax import lax
from jax.sharding import PartitionSpec as P

BLOCK = 64
EPSILON = 1e-06
HIGHEST = lax.Precision.HIGHEST


def shifted(value, axis, steps):
    count = lax.axis_size(axis)
    first, last = (max(0, -steps), min(count, count - steps))
    return lax.ppermute(value, axis, [(source, source + steps) for source in range(first, last)])


def entering(shard, axis, join, neutral):
    place = lax.axis_index(axis)
    gathered = jax.tree.map(
        lambda a, kind: lax.all_gather(a.astype(kind), axis), shard, (jnp.bfloat16, jnp.bfloat16)
    )
    state = jax.tree.map(lambda a, e: jnp.zeros_like(a) + jnp.asarray(e, a.dtype), shard, neutral)

    def one(step, state):
        return join(
            state,
            jax.tree.map(
                lambda a, own: lax.dynamic_index_in_dim(a, step, 0, False).astype(own.dtype),
                gathered,
                shard,
            ),
        )

    return lax.fori_loop(0, place, one, state)


def rms_scale(values, gain):
    return values * lax.rsqrt(jnp.mean(values * values, axis=-1, keepdims=True) + EPSILON) * gain


def join_state(earlier, later):
    decay_one, state_one = earlier
    decay_two, state_two = later
    return (decay_one * decay_two, decay_two[..., None] * state_one + state_two)


def body(
    tokens,
    input_norm_gain,
    pooling_input_weight,
    query_weight,
    forget_weight,
    value_weight,
    pooling_group_maps,
    pooling_scale,
    lower_bound_logits,
    decay_spike,
    head_norm_gain,
    pooling_output_weight,
    recurrent_output_weight,
):
    gathered = lax.all_gather(tokens, "tp", axis=1, tiled=True)[0]
    length_total = gathered.shape[0]
    normed = rms_scale(gathered.astype(jnp.float32), input_norm_gain).astype(jnp.bfloat16)
    pool_width = pooling_input_weight.shape[1]
    rec_width = query_weight.shape[1]
    stacked = jnp.concatenate(
        [pooling_input_weight, query_weight, forget_weight, value_weight], axis=1
    )
    out_local = jnp.concatenate([pooling_output_weight, recurrent_output_weight], axis=0)
    groups_fs = lax.axis_size("fs")
    member = lax.axis_index("fs")
    slice_width = stacked.shape[1] // groups_fs
    own_slice = lax.dynamic_slice_in_dim(stacked, member * slice_width, slice_width, 1)
    column_part = lax.all_gather(own_slice, "sp", axis=0, tiled=True)
    full_input = lax.all_gather(column_part, "fs", axis=1, tiled=True)
    projected = jnp.dot(normed, full_input, preferred_element_type=jnp.float32)
    slice_height = out_local.shape[0] // groups_fs
    own_rows = lax.dynamic_slice_in_dim(out_local, member * slice_height, slice_height, 0)
    row_part = lax.all_gather(own_rows, "sp", axis=1, tiled=True)
    out_full = lax.all_gather(row_part, "fs", axis=0, tiled=True)
    rounded = lax.optimization_barrier(projected.astype(jnp.bfloat16))
    pool_input = rounded[:, :pool_width]
    query_matrix = rounded[:, pool_width : pool_width + rec_width].astype(jnp.float32)
    forget_gate_logit = rounded[:, pool_width + rec_width : pool_width + 2 * rec_width].astype(
        jnp.float32
    )
    value_projected = rounded[:, pool_width + 2 * rec_width :].astype(jnp.float32)
    groups_local = pooling_group_maps.shape[0]
    group_size = pooling_group_maps.shape[1]
    reach_rows = 2 ** (groups_local * lax.axis_size("tp"))
    previous = shifted(pool_input[length_total - reach_rows :], "sp", 1)
    extended = jnp.concatenate([previous, pool_input], axis=0).astype(jnp.float32)
    extended = extended.reshape(reach_rows + length_total, groups_local, group_size)
    group_ids = lax.axis_index("tp") * groups_local + jnp.arange(groups_local, dtype=jnp.int32)
    windows = jnp.left_shift(jnp.int32(2), group_ids)
    window_sum = jnp.zeros((length_total, groups_local, group_size), jnp.float32)
    for offset in range(reach_rows):
        inside = (offset < windows).astype(jnp.float32)
        window_sum = (
            window_sum
            + extended[reach_rows - offset : reach_rows - offset + length_total] * inside[:, None]
        )
    position_index = lax.axis_index("sp") * length_total + jnp.arange(length_total, dtype=jnp.int32)
    counts = jnp.minimum(position_index[:, None] + 1, windows[None, :]).astype(jnp.float32)
    pool_diff = (window_sum / counts[:, :, None] - extended[reach_rows:]).astype(jnp.bfloat16)
    pool_mapped = jnp.einsum(
        "tgc,gcd->tgd", pool_diff, pooling_group_maps, preferred_element_type=jnp.float32
    )
    pool_out = (pool_mapped.reshape(length_total, pool_width) * pooling_scale).astype(jnp.bfloat16)
    local_heads = decay_spike.shape[2]
    head_width = rec_width // local_heads
    blocks = length_total // BLOCK
    block_layout = (blocks, BLOCK, local_heads, head_width)
    reader = jax.nn.silu(query_matrix).reshape(block_layout)
    key_gate_value = jax.nn.sigmoid(-lower_bound_logits) * jax.nn.sigmoid(-forget_gate_logit)
    decay_logarithm = (
        jnp.log1p(-key_gate_value).reshape(length_total, local_heads, head_width)
        + decay_spike[0][:, :, None]
    ).reshape(block_layout)
    key_rows = key_gate_value.reshape(block_layout)
    value_rows = value_projected.reshape(block_layout)
    inner_log = jnp.cumsum(decay_logarithm, axis=1)
    read_scaled = reader * jnp.exp(inner_log)
    key_scaled = key_rows * jnp.exp(-inner_log)
    causal = (jnp.arange(BLOCK)[:, None] >= jnp.arange(BLOCK)[None, :]).astype(jnp.float32)
    scores = jnp.einsum("nthd,nshd->nhts", read_scaled, key_scaled, precision=HIGHEST) * causal
    within = jnp.einsum("nhts,nshe->nthe", scores, value_rows, precision=HIGHEST)
    closing = inner_log[:, -1]
    key_tail = key_rows * jnp.exp(closing[:, None] - inner_log)
    deltas = jnp.einsum("nshd,nshe->nhde", key_tail, value_rows, precision=HIGHEST)
    block_decay = jnp.exp(closing)

    def advance(carried, input_batch):
        decay_now, delta_now = input_batch
        return (decay_now[..., None] * carried + delta_now, carried)

    initial = jnp.zeros((local_heads, head_width, head_width), jnp.float32)
    device_state, entry_states = lax.scan(advance, initial, (block_decay, deltas))
    device_decay = jnp.exp(jnp.sum(closing, axis=0))
    scanned = entering(
        (device_decay, device_state),
        "sp",
        join_state,
        (jnp.ones_like(device_decay), jnp.zeros_like(device_state)),
    )
    prior_state = scanned[1]
    before = jnp.cumsum(closing, axis=0) - closing
    start_states = entry_states + jnp.exp(before)[..., None] * prior_state[None]
    read_out = within + jnp.einsum("nthd,nhde->nthe", read_scaled, start_states, precision=HIGHEST)
    read_out = read_out.reshape(length_total, local_heads, head_width)
    recurrent_output = (
        rms_scale(read_out, 1.0).reshape(length_total, rec_width) * head_norm_gain
    ).astype(jnp.bfloat16)
    mixed_rows = jnp.concatenate([pool_out, recurrent_output], axis=1)
    summed = lax.psum_scatter(
        jnp.dot(mixed_rows, out_full, preferred_element_type=jnp.float32).astype(jnp.bfloat16),
        "tp",
        scatter_dimension=0,
        tiled=True,
    )
    return summed[None]


def solution(mesh):
    placed = (
        P("fs", ("sp", "tp"), None),
        P(),
        P("sp", "tp"),
        P("sp", "tp"),
        P("sp", "tp"),
        P("sp", "tp"),
        P("tp", None, None),
        P("tp"),
        P("tp"),
        P("fs", "sp", "tp"),
        P("tp"),
        P("tp", "sp"),
        P("tp", "sp"),
    )
    return jax.shard_map(
        body, mesh=mesh, in_specs=placed, out_specs=P("fs", ("sp", "tp"), None), check_vma=False
    )
```

profile of v0, /device:TPU:0, one launch (start us, length us, event | category | flops | bytes accessed | tf_op | source)
XLA Modules:
  0.0 247.2 jit_solution(11630460486678041191)
XLA Ops:
  6.5 0.0 all-gather.8.cloned.1.call-start
  6.6 2.3 fusion.8
  8.9 0.0 all-gather.8.cloned.1.call-update
  8.9 0.0 all-gather.12.cloned.1.call-start
  9.0 1.8 fusion.17
  10.8 0.0 all-gather.12.cloned.1.call-update
  10.9 0.0 all-gather.10.cloned.1.call-start
  10.9 46.6 %all-gather.8.cloned.1.call-done = bf16[2048,512]{1,0:T(8,128)(2,1)} async-done(((bf16[512,512]{1,0:T(8,128)(2,1)}), bf16[2048,512]{1,0:T(8,128)(2,1)}) %all-gather.8.cloned.1.call-update) | async-done | bytes 2097168 | tf_op jit(solution)/shard_map/all_gather | solution.py:75
  57.5 0.0 all-gather.10.cloned.1.call-update
  57.5 0.0 all-gather.14.cloned.1.call-start
  57.6 0.1 copy.116
  57.9 2.2 all_gather.25
  60.1 0.2 fusion.2
  60.3 0.1 minimum_convert_fusion
  60.3 25.6 %all-gather.12.cloned.1.call-done = bf16[256,2048]{1,0:T(8,128)(2,1)} async-done(((bf16[256,512]{1,0:T(8,128)(2,1)}), bf16[256,2048]{1,0:T(8,128)(2,1)}) %all-gather.12.cloned.1.call-update) | async-done | bytes 1048592 | tf_op jit(solution)/shard_map/all_gather | solution.py:80
  85.9 0.0 all-gather.14.cloned.1.call-update
  85.9 0.0 reduce-scatter.2.cloned.1.call-start
  86.0 88.5 %all-gather.10.cloned.1.call-done = bf16[2048,2048]{1,0:T(8,128)(2,1)} async-done(((bf16[2048,512]{1,0:T(8,128)(2,1)}), bf16[2048,2048]{1,0:T(8,128)(2,1)}) %all-gather.10.cloned.1.call-update) | async-done | bytes 8388624 | tf_op jit(solution)/shard_map/all_gather | solution.py:76
  174.5 4.7 %convolution_convert_fusion = bf16[128,2048]{1,0:T(8,128)(2,1)S(1)} fusion(bf16[2048,2048]{1,0:T(8,128)(2,1)} %all-gather.10.cloned.1.call-done, bf16[1,128,2048]{2,1,0:T(8,128)(2,1)S(1)} %all_gather.25, f32[2048]{0:T(1024)S(1)} %copy-done.2, f32[128]{0:T(128)S(1)} %add_rsqrt_fusion.1), kind=kOutput, calls=%fused_computation.5 | convolution fusion | flops 1075052544 | bytes 9445888 | tf_op jit(solution)/shard_map/dot_general | solution.py:77
  179.2 3.4 %collective-permute-start = (bf16[16,512]{1,0:T(8,128)(2,1)S(1)}, bf16[16,512]{1,0:T(8,128)(2,1)S(1)}, u32[]{:S(2)}, u32[]{:S(2)}) collective-permute-start(bf16[16,512]{1,0:T(8,128)(2,1)S(1)} %slice.154), channel_id=1, source_target_pairs={{0,8},{8,16},{16,24},{1,9},{9,17},{17,25},{2,10},{10,18},{18,26},{... | collective-permute-start | bytes 49160 | tf_op jit(solution)/shard_map/ppermute | solution.py:14
  182.6 0.2 negate_log-plus-one_fusion
  182.8 0.1 reshape.233
  182.9 0.1 reshape.232
  183.0 0.1 reshape.234
  183.2 0.2 fusion.46
  183.4 0.2 exponential_multiply_fusion
  183.6 0.6 fusion.41
  184.2 0.5 while.26
  184.3 0.2 bitcast_add_fusion.2
  184.5 0.2 bitcast_add_fusion.2
  184.8 9.1 %all-gather.2 = bf16[4,4,128]{2,1,0:T(4,128)(2,1)S(1)} all-gather(bf16[1,4,128]{2,1,0:T(4,128)(2,1)S(1)} %fusion.57), channel_id=2, replica_groups=mesh['sp'=4,'fs'=4,'tp'=2] {'sp'}, dimensions={0}, use_global_device_ids=true | all-gather | bytes 5120 | tf_op jit(solution)/shard_map/all_gather | solution.py:20
  193.8 14.9 %all-gather.1 = bf16[16,128,128]{2,1,0:T(8,128)(2,1)S(1)} all-gather(bf16[4,128,128]{2,1,0:T(8,128)(2,1)S(1)} %convert_element_type.223), channel_id=3, replica_groups=mesh['sp'=4,'fs'=4,'tp'=2] {'sp'}, dimensions={0}, use_global_device_ids=true | all-gather | bytes 655360 | tf_op jit(solution)/shard_map/all_gather | solution.py:20
  208.7 0.5 convolution_multiply_fusion
  209.3 0.3 fusion.54
  209.6 0.8 multiply_reduce_fusion
  210.4 0.3 copy.117
  210.7 0.3 reshape.244
  211.0 0.1 rsqrt.21
  211.1 0.1 fusion.39
  211.3 0.5 fusion.61
  211.8 0.5 convolution_bitcast_fusion
  212.3 0.1 copy.105
  212.4 0.0 copy-done.4
  212.4 0.1 fusion.40
  212.6 16.2 %all-gather.14.cloned.1.call-done = bf16[1024,2048]{1,0:T(8,128)(2,1)} async-done(((bf16[256,2048]{1,0:T(8,128)(2,1)}), bf16[1024,2048]{1,0:T(8,128)(2,1)}) %all-gather.14.cloned.1.call-update) | async-done | bytes 4194320 | tf_op jit(solution)/shard_map/all_gather | solution.py:81
  228.8 3.7 %convolution_convert_fusion.1 = bf16[128,2048]{1,0:T(8,128)(2,1)} fusion(bf16[1024,2048]{1,0:T(8,128)(2,1)} %all-gather.14.cloned.1.call-done, bf16[128,512]{0,1:T(8,128)(2,1)S(1)} %fusion.39, bf16[128,512]{0,1:T(8,128)(2,1)S(1)} %fusion.40), kind=kOutput, calls=%fused_computation.6 | convolution fusion | flops 537657344 | bytes 4980736 | tf_op jit(solution)/shard_map/dot_general | solution.py:157
  232.5 0.0 reduce-scatter.2.cloned.1.call-update
  232.5 8.1 %reduce-scatter.2.cloned.1.call-done = bf16[64,2048]{1,0:T(8,128)(2,1)} async-done(((bf16[128,2048]{1,0:T(8,128)(2,1)}), bf16[64,2048]{1,0:T(8,128)(2,1)}) %reduce-scatter.2.cloned.1.call-update) | async-done | bytes 262160 | tf_op jit(solution)/shard_map/reduce_scatter | solution.py:156
  (46 shorter events, 0.4 us)
Async XLA Ops:
  6.5 205.2 %copy-start = (bf16[2,256,256]{2,1,0:T(8,128)(2,1)S(1)}, bf16[2,256,256]{2,1,0:T(8,128)(2,1)}, u32[]{:S(2)}) copy-start(bf16[2,256,256]{2,1,0:T(8,128)(2,1)} %param.23) | copy-start | bytes 786436
  6.5 51.1 %copy-start.5 = (f32[1,128,4]{1,2,0:T(4,128)S(1)}, f32[1,128,4]{1,2,0:T(4,128)}, u32[]{:S(2)}) copy-start(f32[1,128,4]{1,2,0:T(4,128)} %param.26) | copy-start | bytes 6148
  6.5 51.3 %copy-start.1 = (bf16[1,64,2048]{2,1,0:T(8,128)(2,1)S(1)}, bf16[1,64,2048]{2,1,0:T(8,128)(2,1)}, u32[]{:S(2)}) copy-start(bf16[1,64,2048]{2,1,0:T(8,128)(2,1)} %param.17) | copy-start | bytes 786436
  6.5 53.8 %copy-start.6 = (f32[512]{0:T(512)S(1)}, f32[512]{0:T(512)}, u32[]{:S(2)}) copy-start(f32[512]{0:T(512)} %param.25) | copy-start | bytes 6148
  6.5 51.0 %all-gather.8.cloned.1.call-start = ((), (), s32[]{:S(2)}) async-start(), calls=%async_computation.1 | async-start | bytes 2621440 | tf_op jit(solution)/shard_map/all_gather | solution.py:75
  6.6 167.9 %copy-start.2 = (f32[2048]{0:T(1024)S(1)}, f32[2048]{0:T(1024)}, u32[]{:S(2)}) copy-start(f32[2048]{0:T(1024)} %param.18) | copy-start | bytes 24580
  8.9 77.0 %all-gather.12.cloned.1.call-start = ((), (), s32[]{:S(2)}) async-start(), calls=%async_computation.3 | async-start | bytes 1310720 | tf_op jit(solution)/shard_map/all_gather | solution.py:80
  10.9 163.6 %all-gather.10.cloned.1.call-start = ((), (), s32[]{:S(2)}) async-start(), calls=%async_computation.2 | async-start | bytes 10485760 | tf_op jit(solution)/shard_map/all_gather | solution.py:76
  57.5 171.3 %all-gather.14.cloned.1.call-start = ((), (), s32[]{:S(2)}) async-start(), calls=%async_computation.4 | async-start | bytes 5242880 | tf_op jit(solution)/shard_map/all_gather | solution.py:81
  85.9 154.7 %reduce-scatter.2.cloned.1.call-start = ((), (), s32[]{:S(2)}) async-start(), calls=%async_computation.5 | async-start | bytes 786432 | tf_op jit(solution)/shard_map/reduce_scatter | solution.py:156
  179.2 32.0 %collective-permute-start = (bf16[16,512]{1,0:T(8,128)(2,1)S(1)}, bf16[16,512]{1,0:T(8,128)(2,1)S(1)}, u32[]{:S(2)}, u32[]{:S(2)}) collective-permute-start(bf16[16,512]{1,0:T(8,128)(2,1)S(1)} %slice.154), channel_id=1, source_target_pairs={{0,8},{8,16},{16,24},{1,9},{9,17},{17,25},{2,10},{10,18},{18,26},{... | collective-permute-start | bytes 49160 | tf_op jit(solution)/shard_map/ppermute | solution.py:14
  208.7 2.4 copy-start.3
  211.8 0.7 copy-start.4
Sparse Core Ops, SparseCore 0:
  9.1 48.4 all-gather.7
  59.1 26.7 all-gather.11
  87.7 86.7 all-gather.9
  176.2 52.5 all-gather.13
  232.7 7.9 reduce-scatter.1
where the time goes:
time: 247 us
  waiting for transfers between devices  185 us (75%)
  blocking collectives  26.1 us (11%)
  between operations  13.5 us (5%)
  matrix products  11.1 us (4%)
  other arithmetic  5.86 us (2%)
  starting transfers between devices  3.58 us (1%)
    all_gather x1, waiting for transfers between devices, body(): full_input = lax.all_gather(column_part, 'fs', axis=1, tiled=True)  88.5 us
    all_gather x1, waiting for transfers between devices, body(): column_part = lax.all_gather(own_slice, 'sp', axis=0, tiled=True)  46.6 us
    all_gather x1, waiting for transfers between devices, body(): row_part = lax.all_gather(own_rows, 'sp', axis=1, tiled=True)  25.6 us
    all_gather x2, blocking collectives, entering(): lax.all_gather(a.astype(kind), axis)  23.9 us
    all_gather x1, waiting for transfers between devices, body(): out_full = lax.all_gather(row_part, 'fs', axis=0, tiled=True)  16.2 us
    reduce_scatter x1, waiting for transfers between devices, body(): lax.psum_scatter(jnp.dot(mixed_rows, out_full, preferred_element_type=jnp...  8.08 us
  transfers between devices with their start and end apart: 6, of which 5 were waited for; matrix products, arithmetic and copies ran while one was open for 5% of the time, Pallas kernels for 0%

commit v1 on v0

--- a/solution.py
+++ b/solution.py
@@ -72,7 +72,18 @@
     member = lax.axis_index("fs")
     slice_width = stacked.shape[1] // groups_fs
     own_slice = lax.dynamic_slice_in_dim(stacked, member * slice_width, slice_width, 1)
-    column_part = lax.all_gather(own_slice, "sp", axis=0, tiled=True)
+    axis_n = lax.psum(1, "sp")
+    frame_out = sorted(((tick, (tick + 1) % axis_n) for tick in range(axis_n)))
+    a_next = own_slice
+    parts_seen = [a_next]
+    ix = 1
+    while ix < axis_n:
+        a_next = lax.ppermute(a_next, "sp", frame_out)
+        parts_seen.insert(0, a_next)
+        ix = ix + 1
+    k_now = jnp.concatenate(parts_seen, 0)
+    latest = lax.axis_index("sp") + 1
+    column_part = jnp.roll(k_now, latest * own_slice.shape[0], 0)
     full_input = lax.all_gather(column_part, "fs", axis=1, tiled=True)
     projected = jnp.dot(normed, full_input, preferred_element_type=jnp.float32)
     slice_height = out_local.shape[0] // groups_fs

time: 247 us -> 233 us (0.943)
  waiting for transfers between devices: 185 us -> 166 us
  starting transfers between devices: 3.58 us -> 6.62 us
    all_gather x1 -> x0, waiting for transfers between devices: 46.6 us -> none  [body(): column_part = lax.all_gather(own_slice, 'sp', axis=0, tiled=True)]
    ppermute x0 -> x3, waiting for transfers between devices: none -> 41 us  [body(): a_next = lax.ppermute(a_next, 'sp', frame_out)]
    all_gather x1, waiting for transfers between devices: 25.6 us -> 12.4 us  [body(): row_part = lax.all_gather(own_rows, 'sp', axis=1, tiled=True)]
    ppermute x0 -> x3, starting transfers between devices: none -> 3.11 us  [body(): a_next = lax.ppermute(a_next, 'sp', frame_out)]
  transfers between devices with their start and end apart: 6 -> 8, of which waited for: 5 -> 7; matrix products, arithmetic and copies ran while one was open for 5% -> 6% of each run, Pallas kernels for 0% -> 0%
where the time goes in v1:
time: 233 us
  waiting for transfers between devices  166 us (71%)
  blocking collectives  26.1 us (11%)
  between operations  13.6 us (6%)
  matrix products  11.1 us (5%)
  starting transfers between devices  6.62 us (3%)
  other arithmetic  5.02 us (2%)
  local copies, waits for them, and re-layouts  3.58 us (2%)
    all_gather x1, waiting for transfers between devices, body(): full_input = lax.all_gather(column_part, 'fs', axis=1, tiled=True)  88.5 us
    ppermute x3, waiting for transfers between devices, body(): a_next = lax.ppermute(a_next, 'sp', frame_out)  41 us
    all_gather x2, blocking collectives, entering(): lax.all_gather(a.astype(kind), axis)  23.9 us
    all_gather x1, waiting for transfers between devices, body(): out_full = lax.all_gather(row_part, 'fs', axis=0, tiled=True)  16.4 us
    all_gather x1, waiting for transfers between devices, body(): row_part = lax.all_gather(own_rows, 'sp', axis=1, tiled=True)  12.4 us
    reduce_scatter x1, waiting for transfers between devices, body(): lax.psum_scatter(jnp.dot(mixed_rows, out_full, preferred_element_type=jnp...  8.08 us
    dot_general x1, matrix products, body(): projected = jnp.dot(normed, full_input, preferred_element_type=jnp.float32)  4.69 us
  transfers between devices with their start and end apart: 8, of which 7 were waited for; matrix products, arithmetic and copies ran while one was open for 6% of the time, Pallas kernels for 0%

profile of v1, /device:TPU:0, one launch (start us, length us, event | category | flops | bytes accessed | tf_op | source)
XLA Modules:
  0.0 232.6 jit_solution(1903592280309313660)
XLA Ops:
  6.5 1.5 fusion.8
  8.0 3.1 %collective-permute-start = (bf16[512,512]{1,0:T(8,128)(2,1)S(1)}, bf16[512,512]{1,0:T(8,128)(2,1)S(1)}, u32[]{:S(2)}, u32[]{:S(2)}) collective-permute-start(bf16[512,512]{1,0:T(8,128)(2,1)S(1)} %fusion.8), channel_id=1, source_target_pairs={{0,8},{8,16},{16,24},{24,0},{1,9},{9,17},{17,25},{25,1},{2,10},{10... | collective-permute-start | bytes 1572872 | tf_op jit(solution)/shard_map/ppermute | solution.py:81
  11.1 13.9 %collective-permute-done = bf16[512,512]{1,0:T(8,128)(2,1)S(1)} collective-permute-done((bf16[512,512]{1,0:T(8,128)(2,1)S(1)}, bf16[512,512]{1,0:T(8,128)(2,1)S(1)}, u32[]{:S(2)}, u32[]{:S(2)}) %collective-permute-start) | collective-permute-done | bytes 524320 | tf_op jit(solution)/shard_map/ppermute | solution.py:81
  25.1 14.9 %collective-permute-done.1 = bf16[512,512]{1,0:T(8,128)(2,1)S(1)} collective-permute-done((bf16[512,512]{1,0:T(8,128)(2,1)S(1)}, bf16[512,512]{1,0:T(8,128)(2,1)S(1)}, u32[]{:S(2)}, u32[]{:S(2)}) %collective-permute-start.1) | collective-permute-done | bytes 524320 | tf_op jit(solution)/shard_map/ppermute | solution.py:81
  40.0 1.8 fusion.17
  41.8 0.0 all-gather.9.cloned.1.call-update
  41.8 0.0 all-gather.7.cloned.1.call-start
  41.9 12.2 %collective-permute-done.2 = bf16[512,512]{1,0:T(8,128)(2,1)S(1)} collective-permute-done((bf16[512,512]{1,0:T(8,128)(2,1)S(1)}, bf16[512,512]{1,0:T(8,128)(2,1)S(1)}, u32[]{:S(2)}, u32[]{:S(2)}) %collective-permute-start.2) | collective-permute-done | bytes 524320 | tf_op jit(solution)/shard_map/ppermute | solution.py:81
  54.5 1.5 constant_dynamic-slice_fusion
  55.9 0.0 all-gather.7.cloned.1.call-update
  56.0 0.0 all-gather.11.cloned.1.call-start
  56.0 0.1 copy.116
  56.3 2.2 all_gather.22
  58.5 0.2 fusion.2
  58.7 0.1 minimum_convert_fusion
  58.8 12.4 %all-gather.9.cloned.1.call-done = bf16[256,2048]{1,0:T(8,128)(2,1)} async-done(((bf16[256,512]{1,0:T(8,128)(2,1)}), bf16[256,2048]{1,0:T(8,128)(2,1)}) %all-gather.9.cloned.1.call-update) | async-done | bytes 1048592 | tf_op jit(solution)/shard_map/all_gather | solution.py:91
  71.2 0.0 all-gather.11.cloned.1.call-update
  71.2 0.0 reduce-scatter.2.cloned.1.call-start
  71.3 88.5 %all-gather.7.cloned.1.call-done = bf16[2048,2048]{1,0:T(8,128)(2,1)} async-done(((bf16[2048,512]{1,0:T(8,128)(2,1)}), bf16[2048,2048]{1,0:T(8,128)(2,1)}) %all-gather.7.cloned.1.call-update) | async-done | bytes 8388624 | tf_op jit(solution)/shard_map/all_gather | solution.py:87
  159.8 4.7 %convolution_convert_fusion = bf16[128,2048]{1,0:T(8,128)(2,1)S(1)} fusion(bf16[2048,2048]{1,0:T(8,128)(2,1)} %all-gather.7.cloned.1.call-done, bf16[1,128,2048]{2,1,0:T(8,128)(2,1)S(1)} %all_gather.22, f32[2048]{0:T(1024)S(1)} %copy-done.2, f32[128]{0:T(128)S(1)} %add_rsqrt_fusion.1), kind=kOutput, calls=%fused_computation.5 | convolution fusion | flops 1075052544 | bytes 9445888 | tf_op jit(solution)/shard_map/dot_general | solution.py:88
  164.5 3.4 %collective-permute-start.3 = (bf16[16,512]{1,0:T(8,128)(2,1)S(1)}, bf16[16,512]{1,0:T(8,128)(2,1)S(1)}, u32[]{:S(2)}, u32[]{:S(2)}) collective-permute-start(bf16[16,512]{1,0:T(8,128)(2,1)S(1)} %slice.154), channel_id=1, source_target_pairs={{0,8},{8,16},{16,24},{1,9},{9,17},{17,25},{2,10},{10,18},{18,26},{... | collective-permute-start | bytes 49160 | tf_op jit(solution)/shard_map/ppermute | solution.py:14
  167.9 0.2 negate_log-plus-one_fusion
  168.1 0.1 reshape.233
  168.2 0.1 reshape.232
  168.3 0.1 reshape.234
  168.5 0.2 fusion.46
  168.7 0.2 exponential_multiply_fusion
  168.9 0.6 fusion.41
  169.5 0.5 while.26
  169.6 0.2 bitcast_add_fusion.2
  169.8 0.2 bitcast_add_fusion.2
  170.1 9.1 %all-gather.2 = bf16[4,4,128]{2,1,0:T(4,128)(2,1)S(1)} all-gather(bf16[1,4,128]{2,1,0:T(4,128)(2,1)S(1)} %fusion.57), channel_id=2, replica_groups=mesh['sp'=4,'fs'=4,'tp'=2] {'sp'}, dimensions={0}, use_global_device_ids=true | all-gather | bytes 5120 | tf_op jit(solution)/shard_map/all_gather | solution.py:20
  179.1 14.9 %all-gather.1 = bf16[16,128,128]{2,1,0:T(8,128)(2,1)S(1)} all-gather(bf16[4,128,128]{2,1,0:T(8,128)(2,1)S(1)} %convert_element_type.223), channel_id=3, replica_groups=mesh['sp'=4,'fs'=4,'tp'=2] {'sp'}, dimensions={0}, use_global_device_ids=true | all-gather | bytes 655360 | tf_op jit(solution)/shard_map/all_gather | solution.py:20
  194.0 0.5 convolution_multiply_fusion
  194.6 0.3 fusion.54
  194.9 0.8 multiply_reduce_fusion
  195.7 0.3 copy.117
  196.0 0.3 reshape.244
  196.3 0.1 rsqrt.21
  196.4 0.1 fusion.39
  196.5 0.5 fusion.61
  197.1 0.5 convolution_bitcast_fusion
  197.6 0.1 copy.105
  197.7 0.1 fusion.40
  197.9 16.4 %all-gather.11.cloned.1.call-done = bf16[1024,2048]{1,0:T(8,128)(2,1)} async-done(((bf16[256,2048]{1,0:T(8,128)(2,1)}), bf16[1024,2048]{1,0:T(8,128)(2,1)}) %all-gather.11.cloned.1.call-update) | async-done | bytes 4194320 | tf_op jit(solution)/shard_map/all_gather | solution.py:92
  214.2 3.7 %convolution_convert_fusion.1 = bf16[128,2048]{1,0:T(8,128)(2,1)} fusion(bf16[1024,2048]{1,0:T(8,128)(2,1)} %all-gather.11.cloned.1.call-done, bf16[128,512]{0,1:T(8,128)(2,1)S(1)} %fusion.39, bf16[128,512]{0,1:T(8,128)(2,1)S(1)} %fusion.40), kind=kOutput, calls=%fused_computation.6 | convolution fusion | flops 537657344 | bytes 4980736 | tf_op jit(solution)/shard_map/dot_general | solution.py:168
  218.0 0.0 reduce-scatter.2.cloned.1.call-update
  218.0 8.1 %reduce-scatter.2.cloned.1.call-done = bf16[64,2048]{1,0:T(8,128)(2,1)} async-done(((bf16[128,2048]{1,0:T(8,128)(2,1)}), bf16[64,2048]{1,0:T(8,128)(2,1)}) %reduce-scatter.2.cloned.1.call-update) | async-done | bytes 262160 | tf_op jit(solution)/shard_map/reduce_scatter | solution.py:167
  (58 shorter events, 0.7 us)
Async XLA Ops:
  6.5 190.5 %copy-start = (bf16[2,256,256]{2,1,0:T(8,128)(2,1)S(1)}, bf16[2,256,256]{2,1,0:T(8,128)(2,1)}, u32[]{:S(2)}) copy-start(bf16[2,256,256]{2,1,0:T(8,128)(2,1)} %param.23) | copy-start | bytes 786436
  6.5 64.7 %all-gather.9.cloned.1.call-start = ((), (), s32[]{:S(2)}) async-start(), calls=%async_computation.2 | async-start | bytes 1310720 | tf_op jit(solution)/shard_map/all_gather | solution.py:91
  8.0 17.1 %collective-permute-start = (bf16[512,512]{1,0:T(8,128)(2,1)S(1)}, bf16[512,512]{1,0:T(8,128)(2,1)S(1)}, u32[]{:S(2)}, u32[]{:S(2)}) collective-permute-start(bf16[512,512]{1,0:T(8,128)(2,1)S(1)} %fusion.8), channel_id=1, source_target_pairs={{0,8},{8,16},{16,24},{24,0},{1,9},{9,17},{17,25},{25,1},{2,10},{10... | collective-permute-start | bytes 1572872 | tf_op jit(solution)/shard_map/ppermute | solution.py:81
  25.1 14.9 %collective-permute-start.1 = (bf16[512,512]{1,0:T(8,128)(2,1)S(1)}, bf16[512,512]{1,0:T(8,128)(2,1)S(1)}, u32[]{:S(2)}, u32[]{:S(2)}) collective-permute-start(bf16[512,512]{1,0:T(8,128)(2,1)S(1)} %collective-permute-done), channel_id=1, source_target_pairs={{0,8},{8,16},{16,24},{24,0},{1,9},{9,17},{17,25},{25,1},{2,10},{10... | collective-permute-start | bytes 1572872 | tf_op jit(solution)/shard_map/ppermute | solution.py:81
  40.0 14.1 %collective-permute-start.2 = (bf16[512,512]{1,0:T(8,128)(2,1)S(1)}, bf16[512,512]{1,0:T(8,128)(2,1)S(1)}, u32[]{:S(2)}, u32[]{:S(2)}) collective-permute-start(bf16[512,512]{1,0:T(8,128)(2,1)S(1)} %collective-permute-done.1), channel_id=1, source_target_pairs={{0,8},{8,16},{16,24},{24,0},{1,9},{9,17},{17,25},{25,1},{2,10},{10... | collective-permute-start | bytes 1572872 | tf_op jit(solution)/shard_map/ppermute | solution.py:81
  41.8 118.0 %all-gather.7.cloned.1.call-start = ((), (), s32[]{:S(2)}) async-start(), calls=%async_computation.1 | async-start | bytes 10485760 | tf_op jit(solution)/shard_map/all_gather | solution.py:87
  54.3 1.7 copy-start.5
  54.3 2.0 copy-start.1
  54.4 4.4 %copy-start.6 = (f32[512]{0:T(512)S(1)}, f32[512]{0:T(512)}, u32[]{:S(2)}) copy-start(f32[512]{0:T(512)} %param.25) | copy-start | bytes 6148
  54.4 105.3 %copy-start.2 = (f32[2048]{0:T(1024)S(1)}, f32[2048]{0:T(1024)}, u32[]{:S(2)}) copy-start(f32[2048]{0:T(1024)} %param.18) | copy-start | bytes 24580
  56.0 158.3 %all-gather.11.cloned.1.call-start = ((), (), s32[]{:S(2)}) async-start(), calls=%async_computation.3 | async-start | bytes 5242880 | tf_op jit(solution)/shard_map/all_gather | solution.py:92
  71.2 154.9 %reduce-scatter.2.cloned.1.call-start = ((), (), s32[]{:S(2)}) async-start(), calls=%async_computation.4 | async-start | bytes 786432 | tf_op jit(solution)/shard_map/reduce_scatter | solution.py:167
  164.5 32.0 %collective-permute-start.3 = (bf16[16,512]{1,0:T(8,128)(2,1)S(1)}, bf16[16,512]{1,0:T(8,128)(2,1)S(1)}, u32[]{:S(2)}, u32[]{:S(2)}) collective-permute-start(bf16[16,512]{1,0:T(8,128)(2,1)S(1)} %slice.154), channel_id=1, source_target_pairs={{0,8},{8,16},{16,24},{1,9},{9,17},{17,25},{2,10},{10,18},{18,26},{... | collective-permute-start | bytes 49160 | tf_op jit(solution)/shard_map/ppermute | solution.py:14
  194.0 2.3 %copy-start.3 = (f32[512]{0:T(512)S(1)}, f32[512]{0:T(512)}, u32[]{:S(2)}) copy-start(f32[512]{0:T(512)} %param.27) | copy-start | bytes 6148
  197.0 0.7 copy-start.4
Sparse Core Ops, SparseCore 0:
  41.9 29.2 all-gather.8
  73.0 86.7 all-gather.6
  161.6 52.5 all-gather.10
  218.1 7.9 reduce-scatter.1
